TPU v7x, 32 devices: a whole 2x2x4 slice. The times are simulated.
32 devices in a mesh: grp: 2 (over y), fs: 8 (over z, core), tp: 2 (over x).
Axes of the slice: x: 2, y: 2, z: 4, core: 2. Of those that a mesh axis runs over, the one named last changes fastest.
Arguments:
- prompt: bfloat16 [6144, 2048], P(('grp', 'fs')), parts along dimension 0, may hold values from -6 to 6
- routes: int32 [6144, 4], P(('grp', 'fs')), parts along dimension 0, may hold values from 0 to 7, all different within a row; in each aligned block of 384 rows (0 to 383, 384 to 767, ...) at most 240 rows name the same one
- route_weight: float32 [6144, 4], P(('grp', 'fs')), parts along dimension 0, may hold values from 0.2 to 1
- norm_gain: float32 [2048], P('fs'), may hold values from 0.1 to 1.9
- gate_train: float32 [8, 2048, 1024], P(None, 'fs', 'tp'), may hold values from -0.4 to 0.4
- up_train: float32 [8, 2048, 1024], P(None, 'fs', 'tp'), may hold values from -0.4 to 0.4
- down_train: float32 [8, 1024, 2048], P(None, 'fs', 'tp'), may hold values from -0.07 to 0.07
Outputs:
- gate_serve: bfloat16 [16, 2048, 1024], P(('grp', 'fs'), None, 'tp'), parts along dimension 0
- up_serve: bfloat16 [16, 2048, 1024], P(('grp', 'fs'), None, 'tp'), parts along dimension 0
- down_serve: bfloat16 [16, 1024, 2048], P(('grp', 'fs'), 'tp'), parts along dimension 0
- mixed: bfloat16 [6144, 2048], P(('grp', 'fs'), 'tp'), parts along dimension 0
There are 2 independent parts, one for each index of `grp`. A program takes and returns all parts, laid end to end along the dimension named above; an argument that names none is the same for every part. Nothing has to cross between parts.
Inputs may be any that keep to these rules, and one draw needn't show every extreme that they name: `routes`: each row names 4 different experts. Among the rows of one index of fs no expert is named more than 240 times, a bound that some block reaches on some index.
All inputs are finite; a program needn't handle non-finite values.
Results may differ from a plain program's by a relative error of at most 0.012.
Values may be sent and summed in bfloat16 or wider, within the bound.
No kernel may reach another device: no remote copies, remote signals or barrier semaphores. Data moves between devices by JAX's collectives and lax.ppermute only.
A program may use at most 128 MiB of HBM per device.

v0:
```python
import jax
import jax.numpy as jnp
from jax import lax
from jax.sharding import PartitionSpec as P

TOP = 4
LIMIT = 7.0
ALPHA = 1.702
EPS = 1e-06


def shards(prompt, routes, route_weight, norm_gain, gate_train, up_train, down_train):
    gate_cast = (norm_gain[None, :, None] * gate_train).astype(jnp.bfloat16)
    up_cast = (norm_gain[None, :, None] * up_train).astype(jnp.bfloat16)
    down_cast = down_train.astype(jnp.bfloat16)
    gate_mine, up_mine = (
        lax.all_to_all(gate_cast, "fs", split_axis=0, concat_axis=1, tiled=True),
        lax.all_to_all(up_cast, "fs", split_axis=0, concat_axis=1, tiled=True),
    )
    down_rows = lax.all_to_all(down_cast, "fs", split_axis=0, concat_axis=1, tiled=True)
    down_mine = lax.all_to_all(down_rows, "tp", split_axis=1, concat_axis=2, tiled=True)
    tok_rows, width = prompt.shape
    experts = gate_train.shape[0]
    quarter = width // lax.axis_size("tp")
    capacity = min(tok_rows, max(2, 5 * tok_rows * TOP // (4 * experts)))
    values = prompt.astype(jnp.float32)
    normed = (values * lax.rsqrt(jnp.mean(values * values, axis=-1, keepdims=True) + EPS)).astype(
        jnp.bfloat16
    )
    flat_expert = routes.reshape(-1)
    onehot = (flat_expert[:, None] == jnp.arange(experts, dtype=jnp.int32)[None, :]).astype(
        jnp.int32
    )
    earlier = jnp.cumsum(onehot, axis=0) - onehot
    slot_pos = jnp.sum(earlier * onehot, axis=1)
    target = flat_expert * capacity + slot_pos
    source_row = jnp.arange(tok_rows * TOP, dtype=jnp.int32) // TOP
    outbox = jnp.zeros((experts * capacity, width), jnp.bfloat16).at[target].set(normed[source_row])
    inbox = lax.all_to_all(
        outbox.reshape(experts, capacity, width), "fs", split_axis=0, concat_axis=1, tiled=True
    )
    gate_pre = jnp.einsum("erd,edf->erf", inbox, gate_mine, preferred_element_type=jnp.float32)
    up_pre = jnp.einsum("erd,edf->erf", inbox, up_mine, preferred_element_type=jnp.float32)
    gate_pre = jnp.minimum(gate_pre, LIMIT)
    up_pre = jnp.clip(up_pre, -LIMIT, LIMIT)
    hidden = ((up_pre + 1.0) * gate_pre * jax.nn.sigmoid(ALPHA * gate_pre)).astype(jnp.bfloat16)
    own_width = hidden.shape[2]
    empty = jnp.zeros((hidden.shape[0], hidden.shape[1], down_rows.shape[2]), jnp.float32)
    total = empty
    piece = lax.all_gather(hidden, "tp", axis=2, tiled=True)
    for index in range(piece.shape[2] // own_width):
        cols = piece[:, :, index * own_width : (index + 1) * own_width]
        weight_rows = lax.dynamic_slice_in_dim(down_rows, index * own_width, own_width, 1)
        part = jnp.einsum(
            "erf,efd->erd", cols, weight_rows, preferred_element_type=jnp.float32
        ).astype(jnp.bfloat16)
        total = total + part.astype(jnp.float32)
    summed = total.astype(jnp.bfloat16)
    back = lax.all_to_all(summed, "fs", split_axis=1, concat_axis=0, tiled=True)
    picked = back.reshape(experts * capacity, quarter)[target].astype(jnp.float32)
    weighted = picked.reshape(tok_rows, TOP, quarter) * route_weight[:, :, None]
    mixed = jnp.sum(weighted, axis=1).astype(jnp.bfloat16)
    return (gate_mine, up_mine, down_mine, mixed)


def solution(mesh):
    return jax.shard_map(
        shards,
        mesh=mesh,
        in_specs=(
            P(("grp", "fs"), None),
            P(("grp", "fs"), None),
            P(("grp", "fs"), None),
            P("fs"),
            P(None, "fs", "tp"),
            P(None, "fs", "tp"),
            P(None, "fs", "tp"),
        ),
        out_specs=(
            P(("grp", "fs"), None, "tp"),
            P(("grp", "fs"), None, "tp"),
            P(("grp", "fs"), "tp", None),
            P(("grp", "fs"), "tp"),
        ),
        check_vma=False,
    )
```

profile of v0, /device:TPU:0, one launch (start us, length us, event | category | flops | bytes accessed | tf_op | source)
XLA Modules:
  0.0 601.2 jit_solution(9907944391653193153)
XLA Ops:
  7.2 6.8 %multiply_convert_fusion = (bf16[8,256,512]{2,1,0:T(8,128)(2,1)}, bf16[8,256,512]{2,1,0:T(8,128)(2,1)}) fusion(f32[8,256,512]{2,1,0:T(8,128)} %param.12, f32[256]{0:T(256)} %param.10, f32[8,256,512]{2,1,0:T(8,128)} %param.11), kind=kLoop, calls=%fused_computation.7 | loop fusion | flops 4194304 | bytes 12583936 | tf_op jit(solution)/shard_map/convert_element_type | solution.py:14
  14.0 0.0 copy-start.4
  14.0 6.5 %all-to-all-start = ((bf16[8,256,512]{2,1,0:T(8,128)(2,1)}), bf16[8,256,512]{2,1,0:T(8,128)(2,1)S(1)}, u32[]{:S(2)}, u32[]{:S(2)}) async-start(bf16[8,256,512]{2,1,0:T(8,128)(2,1)} %get-tuple-element.17), calls=%async_computation | async-start | bytes 4194304 | tf_op jit(solution)/shard_map/all_to_all | solution.py:17
  20.5 0.0 copy-done.4
  20.5 0.1 copy.32
  20.6 0.1 eq.29
  20.8 0.1 eq.25
  20.9 2.3 reduce-window.6
  23.2 0.3 slice_reduce_fusion
  23.5 0.2 reduce-window.9
  23.7 0.1 copy.31
  23.8 0.2 mul.72
  24.0 0.6 fusion.12
  24.6 0.1 add_bitcast_fusion
  24.7 1.8 fusion.4
  26.5 2.9 fusion.5
  29.4 33.0 %scatter_custom_fusion = bf16[1920,2048]{1,0:T(8,128)(2,1)} fusion(s32[1536]{0:T(1024)S(1)} %fusion.11, bf16[384,2048]{1,0:T(8,128)(2,1)} %fusion.5, s32[2048]{0:T(1024)S(1)} %pad_clamp_fusion.1, bf16[]{:T(256)} %constant.17.clone.1), kind=kCustom, calls=%fused_computation.4 | custom fusion | bytes 7864832 | tf_op jit(solution)/shard_map/scatter | solution.py:38
  62.4 7.1 %all-to-all-done = bf16[8,256,512]{2,1,0:T(8,128)(2,1)S(1)} async-done(((bf16[8,256,512]{2,1,0:T(8,128)(2,1)}), bf16[8,256,512]{2,1,0:T(8,128)(2,1)S(1)}, u32[]{:S(2)}, u32[]{:S(2)}) %all-to-all-start) | async-done | bytes 2097184 | tf_op jit(solution)/shard_map/all_to_all | solution.py:17
  69.5 0.0 copy-start.2
  69.5 178.2 %all_to_all.72 = bf16[8,240,2048]{2,1,0:T(8,128)(2,1)} all-to-all(bf16[8,240,2048]{2,1,0:T(8,128)(2,1)} %bitcast.61), channel_id=1, replica_groups=mesh['grp'=2,'fs'=8,'tp'=2] {'fs'}, dimensions={0} | all-to-all | bytes 15728640 | tf_op jit(solution)/shard_map/all_to_all | solution.py:39
  247.7 4.4 all-to-all-start.1
  252.1 0.0 all-gather.3.cloned.1.call-start
  252.1 0.0 copy-done.2
  252.1 9.5 %fusion.13 = f32[1920,512]{1,0:T(8,128)} fusion(bf16[1920,2048]{1,0:T(8,128)(2,1)} %bitcast.73, bf16[2048,512]{1,0:T(8,128)(2,1)S(1)} %bitcast.70), kind=kOutput, calls=%fused_computation.45 | convolution fusion | flops 4026531840 | bytes 13893632 | tf_op jit(solution)/shard_map/erd,edf->erf/dot_general | solution.py:42
  261.6 39.5 %all-to-all-done.1 = bf16[8,256,512]{2,1,0:T(8,128)(2,1)} async-done(((bf16[8,256,512]{2,1,0:T(8,128)(2,1)}), bf16[8,256,512]{2,1,0:T(8,128)(2,1)}, u32[]{:S(2)}, u32[]{:S(2)}) %all-to-all-start.1) | async-done | bytes 2097184 | tf_op jit(solution)/shard_map/all_to_all | solution.py:18
  301.1 11.8 %multiply_convert_fusion.2 = bf16[1920,512]{1,0:T(8,128)(2,1)} fusion(f32[1920,512]{1,0:T(8,128)} %fusion.13, bf16[1920,2048]{1,0:T(8,128)(2,1)} %bitcast.74, bf16[2048,512]{1,0:T(8,128)(2,1)} %bitcast.8), kind=kOutput, calls=%fused_computation.11 | convolution fusion | flops 4036362240 | bytes 15859712 | tf_op jit(solution)/shard_map/erd,edf->erf/dot_general | solution.py:43
  312.9 0.0 all-gather.3.cloned.1.call-update
  312.9 2.5 convert_element_type.62
  315.4 51.7 %all_to_all.73 = bf16[8,128,1024]{2,1,0:T(8,128)(2,1)S(1)} all-to-all(bf16[8,128,1024]{2,1,0:T(8,128)(2,1)S(1)} %convert_element_type.62), channel_id=1, replica_groups=mesh['grp'=2,'fs'=8,'tp'=2] {'fs'}, dimensions={0} | all-to-all | bytes 4194304 | tf_op jit(solution)/shard_map/all_to_all | solution.py:20
  367.1 1.3 copy-done
  368.4 5.2 copy.46
  373.6 0.5 broadcast.146
  374.1 12.8 %reduce.6 = bf16[1024,1024]{1,0:T(8,128)(2,1)S(1)} reduce(bf16[1024,1,1024]{2,1,0:T(2,128)(2,1)} %bitcast.64, bf16[]{:T(256)} %broadcast.146), dimensions={1}, to_apply=%bitcast.58.reduce_sub_computation | reduce | bytes 4194306
  386.9 2.5 reshape.227
  389.4 4.2 all-to-all-start.3
  393.6 0.0 all-gather.3.cloned.1.call-done
  393.6 0.0 copy-start.1
  393.6 0.0 copy-start.6
  393.6 4.2 fusion.6
  397.8 0.0 copy-done.1
  397.8 0.0 copy-done.6
  397.8 2.3 fusion.2
  400.1 27.0 %copy.45 = bf16[1,1920,1024]{2,0,1:T(2,128)(2,1)} copy(bf16[1,1920,1024]{2,1,0:T(8,128)(2,1)S(1)} %fusion.2) | data formatting | bytes 7864320 | tf_op jit(solution)/shard_map/convert_element_type | solution.py:58
  427.1 24.6 %reduce.7 = bf16[1920,1024]{1,0:T(8,128)(2,1)} reduce(bf16[1920,1,1024]{2,1,0:T(2,128)(2,1)} %bitcast.62, bf16[]{:T(256)} %broadcast.146), dimensions={1}, to_apply=%bitcast.57.reduce_sub_computation | reduce | bytes 7864322
  451.7 7.6 %reshape.225 = bf16[8,2,122880]{2,1,0:T(2,128)(2,1)} reshape(bf16[1920,1024]{1,0:T(8,128)(2,1)} %reduce.7) | data formatting | bytes 7864320
  459.3 0.0 copy-start.5
  459.3 0.0 all-to-all-done.3
  459.3 4.8 all-to-all-start.5
  464.2 0.0 copy-done.5
  464.2 0.1 copy.35
  464.3 3.1 reshape.228
  467.4 3.0 copy.37
  470.4 2.6 copy.30
  473.0 3.9 copy.36
  476.9 75.6 %all-to-all-done.5 = bf16[8,2,122880]{2,1,0:T(2,128)(2,1)} async-done(((bf16[8,2,122880]{2,1,0:T(2,128)(2,1)}), bf16[8,2,122880]{2,1,0:T(2,128)(2,1)}, u32[]{:S(2)}, u32[]{:S(2)}) %all-to-all-start.5) | async-done | bytes 3932192 | tf_op jit(solution)/shard_map/all_to_all | solution.py:59
  552.5 8.5 %reshape.226 = bf16[1920,1,1024]{2,1,0:T(2,128)(2,1)} reshape(bf16[8,2,122880]{2,1,0:T(2,128)(2,1)} %all-to-all-done.5) | data formatting | bytes 7864320
  561.0 6.8 %copy.44 = bf16[1,1920,1024]{2,1,0:T(8,128)(2,1)} copy(bf16[1,1920,1024]{2,0,1:T(2,128)(2,1)} %bitcast.63) | data formatting | bytes 7864320
  567.8 9.7 %gather_fusion = bf16[1536,1024]{1,0:T(8,128)(2,1)S(1)} fusion(bf16[1920,1024]{1,0:T(8,128)(2,1)} %bitcast.60, s32[2048]{0:T(1024)S(1)} %pad_clamp_fusion), kind=kCustom, calls=%fused_computation.1 | custom fusion | bytes 6297600 | tf_op jit(solution)/shard_map/gather | solution.py:60
  577.5 4.4 reshape.190
  581.9 0.0 copy-start.3
  581.9 7.9 %multiply_reduce_fusion = bf16[384,1024]{1,0:T(8,128)(2,1)} fusion(f32[384,4,1024]{2,1,0:T(4,128)} %reshape.190, f32[384,4]{1,0:T(8,128)S(1)} %copy.35), kind=kLoop, calls=%fused_computation.6 | loop fusion | flops 2752512 | bytes 7084032 | tf_op jit(solution)/shard_map/reduce_sum | solution.py:62
  589.8 0.0 copy-done.3
  589.8 1.3 copy.49
  591.1 3.0 copy.50
  (8 shorter events, 0.1 us)
Async XLA Ops:
  14.0 6.5 %copy-start.4 = (s32[384,4]{0,1:T(4,128)S(1)}, s32[384,4]{0,1:T(4,128)}, u32[]{:S(2)}) copy-start(s32[384,4]{0,1:T(4,128)} %param.8) | copy-start | bytes 18436
  14.0 55.5 %all-to-all-start = ((bf16[8,256,512]{2,1,0:T(8,128)(2,1)}), bf16[8,256,512]{2,1,0:T(8,128)(2,1)S(1)}, u32[]{:S(2)}, u32[]{:S(2)}) async-start(bf16[8,256,512]{2,1,0:T(8,128)(2,1)} %get-tuple-element.17), calls=%async_computation | async-start | bytes 4194304 | tf_op jit(solution)/shard_map/all_to_all | solution.py:17
  69.5 182.6 %copy-start.2 = (bf16[8,256,512]{2,1,0:T(8,128)(2,1)}, bf16[8,256,512]{2,1,0:T(8,128)(2,1)S(1)}, u32[]{:S(2)}) copy-start(bf16[8,256,512]{2,1,0:T(8,128)(2,1)S(1)} %all-to-all-done) | copy-start | bytes 6291460
  247.7 53.4 %all-to-all-start.1 = ((bf16[8,256,512]{2,1,0:T(8,128)(2,1)}), bf16[8,256,512]{2,1,0:T(8,128)(2,1)}, u32[]{:S(2)}, u32[]{:S(2)}) async-start(bf16[8,256,512]{2,1,0:T(8,128)(2,1)} %get-tuple-element.16), calls=%async_computation.1 | async-start | bytes 4194304 | tf_op jit(solution)/shard_map/all_to_all | solution.py:18
  252.1 141.5 %all-gather.3.cloned.1.call-start = ((), (), s32[]{:S(2)}) async-start(), calls=%async_computation.6 | async-start | bytes 5898240 | tf_op jit(solution)/shard_map/all_gather | solution.py:50
  367.1 1.3 copy-start
  389.4 69.9 %all-to-all-start.3 = ((bf16[2,2,262144]{2,1,0:T(2,128)(2,1)}), bf16[2,2,262144]{2,1,0:T(2,128)(2,1)S(1)}, u32[]{:S(2)}, u32[]{:S(2)}) async-start(bf16[2,2,262144]{2,1,0:T(2,128)(2,1)} %reshape.227), calls=%async_computation.3 | async-start | bytes 4194304 | tf_op jit(solution)/shard_map/all_to_all | solution.py:21
  393.6 4.2 copy-start.1
  393.6 4.2 copy-start.6
  459.3 4.9 copy-start.5
  459.3 93.2 %all-to-all-start.5 = ((bf16[8,2,122880]{2,1,0:T(2,128)(2,1)}), bf16[8,2,122880]{2,1,0:T(2,128)(2,1)}, u32[]{:S(2)}, u32[]{:S(2)}) async-start(bf16[8,2,122880]{2,1,0:T(2,128)(2,1)} %reshape.225), calls=%async_computation.5 | async-start | bytes 7864320 | tf_op jit(solution)/shard_map/all_to_all | solution.py:59
  581.9 7.9 %copy-start.3 = (bf16[8,256,512]{2,1,0:T(8,128)(2,1)S(1)}, bf16[8,256,512]{2,1,0:T(8,128)(2,1)}, u32[]{:S(2)}) copy-start(bf16[8,256,512]{2,1,0:T(8,128)(2,1)} %copy-done.2) | copy-start | bytes 6291460
Sparse Core Ops, SparseCore 0:
  313.0 52.6 all-gather.2
where the time goes:
time: 605 us; the launch traced here: 601 us
  blocking collectives  230 us (38%)
  local copies, waits for them, and re-layouts  125 us (21%)
  waiting for transfers between devices  122 us (20%)
  other arithmetic  62.4 us (10%)
  matrix products  27.7 us (5%)
  starting transfers between devices  19.9 us (3%)
  between operations  14.4 us (2%)
    all_to_all x1, blocking collectives, shards(): lax.all_to_all(outbox.reshape(experts, capacity, width), 'fs', split_axis...  178 us
    all_to_all x1, waiting for transfers between devices, shards(): back = lax.all_to_all(summed, 'fs', split_axis=1, concat_axis=0, tiled=True)  75.6 us
    all_to_all x1, blocking collectives, shards(): lax.all_to_all(down_cast, 'fs', split_axis=0, concat_axis=1, tiled=True)  51.7 us
    unnamed x26, local copies, waits for them, and re-layouts  41.9 us
    all_to_all x1, waiting for transfers between devices, shards(): lax.all_to_all(up_cast, 'fs', split_axis=0, concat_axis=1, tiled=True)  39.5 us
    unnamed x3, other arithmetic  37.4 us
    scatter x1, local copies, waits for them, and re-layouts, shards(): jnp.zeros((experts * capacity, width), jnp.bfloat16).at[target]  33 us
    convert_element_type x1, local copies, waits for them, and re-layouts, shards(): summed = total.astype(jnp.bfloat16)  27 us
  transfers between devices with their start and end apart: 5, of which 3 were waited for; matrix products, arithmetic and copies ran while one was open for 25% of the time, Pallas kernels for 0%

commit v1 on v0

--- a/solution.py
+++ b/solution.py
@@ -2,11 +2,20 @@
 import jax.numpy as jnp
 from jax import lax
 from jax.sharding import PartitionSpec as P
+from jax.lax import all_to_all, axis_size
 
 TOP = 4
 LIMIT = 7.0
 ALPHA = 1.702
 EPS = 1e-06
+
+
+def store_the_frame(patch, row_dim, join_dim):
+    arr_out = axis_size("fs")
+    t1 = jnp.split(patch, arr_out, row_dim)
+    y2 = jnp.stack(t1)
+    state_now = all_to_all(y2, axis_name="fs", split_axis=0, concat_axis=0)
+    return jnp.concatenate(state_now, join_dim)
 
 
 def shards(prompt, routes, route_weight, norm_gain, gate_train, up_train, down_train):
@@ -56,7 +65,7 @@
         ).astype(jnp.bfloat16)
         total = total + part.astype(jnp.float32)
     summed = total.astype(jnp.bfloat16)
-    back = lax.all_to_all(summed, "fs", split_axis=1, concat_axis=0, tiled=True)
+    back = store_the_frame(summed, 1, 0)
     picked = back.reshape(experts * capacity, quarter)[target].astype(jnp.float32)
     weighted = picked.reshape(tok_rows, TOP, quarter) * route_weight[:, :, None]
     mixed = jnp.sum(weighted, axis=1).astype(jnp.bfloat16)

time: 605 us -> 548 us (0.906)
  local copies, waits for them, and re-layouts: 125 us -> 81.6 us
  other arithmetic: 62.4 us -> 37.6 us
  waiting for transfers between devices: 122 us -> 134 us
    convert_element_type x1 -> x0, local copies, waits for them, and re-layouts: 27 us -> none  [shards(): summed = total.astype(jnp.bfloat16)]
    unnamed x3 -> x2, other arithmetic: 37.4 us -> 12.9 us
    unnamed x26 -> x30, local copies, waits for them, and re-layouts: 41.9 us -> 24.8 us
    all_to_all x1, waiting for transfers between devices: 0.01 us -> 11.5 us  [shards(): lax.all_to_all(down_rows, 'tp', split_axis=1, concat_axis=2, tiled=True)]
  transfers between devices with their start and end apart: 5 -> 5, of which waited for: 3 -> 4; matrix products, arithmetic and copies ran while one was open for 25% -> 19% of each run, Pallas kernels for 0% -> 0%
where the time goes in v1:
time: 548 us; the launch traced here: 544 us
  blocking collectives  230 us (42%)
  waiting for transfers between devices  134 us (24%)
  local copies, waits for them, and re-layouts  81.6 us (15%)
  other arithmetic  37.6 us (7%)
  matrix products  27.6 us (5%)
  starting transfers between devices  19.4 us (4%)
  between operations  14.5 us (3%)
    all_to_all x1, blocking collectives, shards(): lax.all_to_all(outbox.reshape(experts, capacity, width), 'fs', split_axis...  178 us
    all_to_all x1, waiting for transfers between devices, store_the_frame(): state_now = all_to_all(y2, axis_name='fs', split_axis=0, concat_axis=0)  75.6 us
    all_to_all x1, blocking collectives, shards(): lax.all_to_all(down_cast, 'fs', split_axis=0, concat_axis=1, tiled=True)  51.6 us
    all_to_all x1, waiting for transfers between devices, shards(): lax.all_to_all(up_cast, 'fs', split_axis=0, concat_axis=1, tiled=True)  39.5 us
    scatter x1, local copies, waits for them, and re-layouts, shards(): jnp.zeros((experts * capacity, width), jnp.bfloat16).at[target]  33.3 us
    unnamed x30, local copies, waits for them, and re-layouts  24.8 us
    unnamed x2, other arithmetic  12.9 us
    dot_general x1, matrix products, shards(): jnp.einsum('erd,edf->erf', inbox, up_mine, preferred_element_type=jnp.flo...  11.7 us
  transfers between devices with their start and end apart: 5, of which 4 were waited for; matrix products, arithmetic and copies ran while one was open for 19% of the time, Pallas kernels for 0%

profile of v1, /device:TPU:0, one launch (start us, length us, event | category | flops | bytes accessed | tf_op | source)
XLA Modules:
  0.0 544.3 jit_solution(15226786300977752887)
XLA Ops:
  7.2 6.8 %multiply_convert_fusion = (bf16[8,256,512]{2,1,0:T(8,128)(2,1)}, bf16[8,256,512]{2,1,0:T(8,128)(2,1)}) fusion(f32[8,256,512]{2,1,0:T(8,128)} %param.12, f32[256]{0:T(256)} %param.10, f32[8,256,512]{2,1,0:T(8,128)} %param.11), kind=kLoop, calls=%fused_computation.7 | loop fusion | flops 4194304 | bytes 12583936 | tf_op jit(solution)/shard_map/convert_element_type | solution.py:23
  14.0 0.0 copy-start.4
  14.0 6.5 %all-to-all-start = ((bf16[8,256,512]{2,1,0:T(8,128)(2,1)}), bf16[8,256,512]{2,1,0:T(8,128)(2,1)S(1)}, u32[]{:S(2)}, u32[]{:S(2)}) async-start(bf16[8,256,512]{2,1,0:T(8,128)(2,1)} %get-tuple-element.17), calls=%async_computation | async-start | bytes 4194304 | tf_op jit(solution)/shard_map/all_to_all | solution.py:26
  20.5 0.0 copy-done.4
  20.5 0.1 copy.31
  20.6 0.1 eq.29
  20.8 0.1 eq.25
  20.9 2.3 reduce-window.6
  23.2 0.3 slice_reduce_fusion
  23.5 0.2 reduce-window.9
  23.7 0.1 copy.30
  23.8 0.2 mul.72
  24.0 0.3 fusion.20
  24.3 0.1 add_bitcast_fusion
  24.5 1.8 fusion.4
  26.3 2.9 fusion.5
  29.2 33.3 %scatter_custom_fusion = bf16[1920,2048]{1,0:T(8,128)(2,1)} fusion(s32[1536]{0:T(1024)S(1)} %fusion.19, bf16[384,2048]{1,0:T(8,128)(2,1)} %fusion.5, s32[2048]{0:T(1024)S(1)} %pad_clamp_fusion.1, bf16[]{:T(256)} %constant.17.clone.1), kind=kCustom, calls=%fused_computation.4 | custom fusion | bytes 7864832 | tf_op jit(solution)/shard_map/scatter | solution.py:47
  62.5 7.0 %all-to-all-done = bf16[8,256,512]{2,1,0:T(8,128)(2,1)S(1)} async-done(((bf16[8,256,512]{2,1,0:T(8,128)(2,1)}), bf16[8,256,512]{2,1,0:T(8,128)(2,1)S(1)}, u32[]{:S(2)}, u32[]{:S(2)}) %all-to-all-start) | async-done | bytes 2097184 | tf_op jit(solution)/shard_map/all_to_all | solution.py:26
  69.5 178.2 %all_to_all.68 = bf16[8,240,2048]{2,1,0:T(8,128)(2,1)} all-to-all(bf16[8,240,2048]{2,1,0:T(8,128)(2,1)} %bitcast.86), channel_id=1, replica_groups=mesh['grp'=2,'fs'=8,'tp'=2] {'fs'}, dimensions={0} | all-to-all | bytes 15728640 | tf_op jit(solution)/shard_map/all_to_all | solution.py:48
  247.7 4.3 all-to-all-start.1
  252.1 0.0 all-gather.3.cloned.1.call-start
  252.1 0.0 copy-done.2
  252.1 9.5 %fusion.21 = f32[1920,512]{1,0:T(8,128)} fusion(bf16[1920,2048]{1,0:T(8,128)(2,1)} %bitcast.96, bf16[2048,512]{1,0:T(8,128)(2,1)S(1)} %bitcast.93), kind=kOutput, calls=%fused_computation.59 | convolution fusion | flops 4026531840 | bytes 13893632 | tf_op jit(solution)/shard_map/erd,edf->erf/dot_general | solution.py:51
  261.6 39.5 %all-to-all-done.1 = bf16[8,256,512]{2,1,0:T(8,128)(2,1)} async-done(((bf16[8,256,512]{2,1,0:T(8,128)(2,1)}), bf16[8,256,512]{2,1,0:T(8,128)(2,1)}, u32[]{:S(2)}, u32[]{:S(2)}) %all-to-all-start.1) | async-done | bytes 2097184 | tf_op jit(solution)/shard_map/all_to_all | solution.py:27
  301.1 11.7 %multiply_convert_fusion.2 = bf16[1920,512]{1,0:T(8,128)(2,1)} fusion(f32[1920,512]{1,0:T(8,128)} %fusion.21, bf16[1920,2048]{1,0:T(8,128)(2,1)} %bitcast.97, bf16[2048,512]{1,0:T(8,128)(2,1)} %bitcast.8), kind=kOutput, calls=%fused_computation.10 | convolution fusion | flops 4036362240 | bytes 15859712 | tf_op jit(solution)/shard_map/erd,edf->erf/dot_general | solution.py:52
  312.8 0.0 all-gather.3.cloned.1.call-update
  312.8 2.5 convert_element_type.62
  315.3 51.6 %all_to_all.69 = bf16[8,128,1024]{2,1,0:T(8,128)(2,1)S(1)} all-to-all(bf16[8,128,1024]{2,1,0:T(8,128)(2,1)S(1)} %convert_element_type.62), channel_id=1, replica_groups=mesh['grp'=2,'fs'=8,'tp'=2] {'fs'}, dimensions={0} | all-to-all | bytes 4194304 | tf_op jit(solution)/shard_map/all_to_all | solution.py:29
  367.0 1.3 copy-done
  368.3 5.2 copy.39
  373.4 0.5 broadcast.146
  373.9 12.8 %reduce.6 = bf16[1024,1024]{1,0:T(8,128)(2,1)S(1)} reduce(bf16[1024,1,1024]{2,1,0:T(2,128)(2,1)} %bitcast.87, bf16[]{:T(256)} %broadcast.146), dimensions={1}, to_apply=%bitcast.84.reduce_sub_computation | reduce | bytes 4194306
  386.7 2.5 reshape.217
  389.2 3.8 all-to-all-start.3
  393.0 0.0 all-gather.3.cloned.1.call-done
  393.0 0.0 copy-start.1
  393.1 0.0 copy-start.6
  393.1 4.2 fusion.6
  397.2 0.0 copy-done.1
  397.3 0.0 copy-done.6
  397.3 2.3 fusion.2
  399.6 0.9 fusion.14
  400.4 0.8 fusion.13
  401.3 0.8 fusion.12
  402.1 0.8 fusion.11
  402.9 0.8 fusion.10
  403.7 0.8 fusion.9
  404.6 0.8 fusion.8
  405.4 0.8 fusion.7
  406.2 11.5 %all-to-all-done.3 = bf16[2,2,262144]{2,1,0:T(2,128)(2,1)S(1)} async-done(((bf16[2,2,262144]{2,1,0:T(2,128)(2,1)}), bf16[2,2,262144]{2,1,0:T(2,128)(2,1)S(1)}, u32[]{:S(2)}, u32[]{:S(2)}) %all-to-all-start.3) | async-done | bytes 2097184 | tf_op jit(solution)/shard_map/all_to_all | solution.py:30
  417.7 4.7 all-to-all-start.5
  422.5 0.0 copy-done.5
  422.5 0.1 copy.33
  422.6 3.1 reshape.218
  425.7 3.0 copy.35
  428.7 2.6 copy.29
  431.3 3.9 copy.34
  435.2 75.6 %all-to-all-done.5 = bf16[8,1,240,1024]{3,2,1,0:T(8,128)(2,1)} async-done(((bf16[8,1,240,1024]{3,2,1,0:T(8,128)(2,1)}), bf16[8,1,240,1024]{3,2,1,0:T(8,128)(2,1)}, u32[]{:S(2)}, u32[]{:S(2)}) %all-to-all-start.5) | async-done | bytes 3932192 | tf_op jit(solution)/shard_map/all_to_all | solution.py:17
  510.8 9.7 %gather_fusion = bf16[1536,1024]{1,0:T(8,128)(2,1)S(1)} fusion(bf16[1920,1024]{1,0:T(8,128)(2,1)} %bitcast.24, s32[2048]{0:T(1024)S(1)} %pad_clamp_fusion), kind=kCustom, calls=%fused_computation.1 | custom fusion | bytes 6297600 | tf_op jit(solution)/shard_map/gather | solution.py:69
  520.6 4.4 reshape.182
  524.9 7.9 %multiply_reduce_fusion = bf16[384,1024]{1,0:T(8,128)(2,1)} fusion(f32[384,4,1024]{2,1,0:T(4,128)} %reshape.182, f32[384,4]{1,0:T(8,128)S(1)} %copy.33), kind=kLoop, calls=%fused_computation.6 | loop fusion | flops 2752512 | bytes 7084032 | tf_op jit(solution)/shard_map/reduce_sum | solution.py:71
  532.8 0.0 copy-done.3
  532.8 1.3 copy.49
  534.1 3.0 copy.50
  (11 shorter events, 0.1 us)
Async XLA Ops:
  14.0 6.5 %copy-start.4 = (s32[384,4]{0,1:T(4,128)S(1)}, s32[384,4]{0,1:T(4,128)}, u32[]{:S(2)}) copy-start(s32[384,4]{0,1:T(4,128)} %param.8) | copy-start | bytes 18436
  14.0 55.5 %all-to-all-start = ((bf16[8,256,512]{2,1,0:T(8,128)(2,1)}), bf16[8,256,512]{2,1,0:T(8,128)(2,1)S(1)}, u32[]{:S(2)}, u32[]{:S(2)}) async-start(bf16[8,256,512]{2,1,0:T(8,128)(2,1)} %get-tuple-element.17), calls=%async_computation | async-start | bytes 4194304 | tf_op jit(solution)/shard_map/all_to_all | solution.py:26
  69.5 182.6 %copy-start.2 = (bf16[8,256,512]{2,1,0:T(8,128)(2,1)}, bf16[8,256,512]{2,1,0:T(8,128)(2,1)S(1)}, u32[]{:S(2)}) copy-start(bf16[8,256,512]{2,1,0:T(8,128)(2,1)S(1)} %all-to-all-done) | copy-start | bytes 6291460
  247.7 53.4 %all-to-all-start.1 = ((bf16[8,256,512]{2,1,0:T(8,128)(2,1)}), bf16[8,256,512]{2,1,0:T(8,128)(2,1)}, u32[]{:S(2)}, u32[]{:S(2)}) async-start(bf16[8,256,512]{2,1,0:T(8,128)(2,1)} %get-tuple-element.16), calls=%async_computation.1 | async-start | bytes 4194304 | tf_op jit(solution)/shard_map/all_to_all | solution.py:27
  252.1 141.0 %all-gather.3.cloned.1.call-start = ((), (), s32[]{:S(2)}) async-start(), calls=%async_computation.6 | async-start | bytes 5898240 | tf_op jit(solution)/shard_map/all_gather | solution.py:59
  367.0 1.3 copy-start
  389.2 28.5 %all-to-all-start.3 = ((bf16[2,2,262144]{2,1,0:T(2,128)(2,1)}), bf16[2,2,262144]{2,1,0:T(2,128)(2,1)S(1)}, u32[]{:S(2)}, u32[]{:S(2)}) async-start(bf16[2,2,262144]{2,1,0:T(2,128)(2,1)} %reshape.217), calls=%async_computation.3 | async-start | bytes 4194304 | tf_op jit(solution)/shard_map/all_to_all | solution.py:30
  393.0 4.2 copy-start.1
  393.1 4.2 copy-start.6
  406.2 16.3 %copy-start.5 = (f32[384,4]{0,1:T(4,128)S(1)}, f32[384,4]{0,1:T(4,128)}, u32[]{:S(2)}) copy-start(f32[384,4]{0,1:T(4,128)} %param.9) | copy-start | bytes 18436
  417.7 93.1 %all-to-all-start.5 = ((bf16[8,1,240,1024]{3,2,1,0:T(8,128)(2,1)}), bf16[8,1,240,1024]{3,2,1,0:T(8,128)(2,1)}, u32[]{:S(2)}, u32[]{:S(2)}) async-start(bf16[8,1,240,1024]{3,2,1,0:T(8,128)(2,1)} %fusion.7), calls=%async_computation.5 | async-start | bytes 7864320 | tf_op jit(solution)/shard_map/all_to_all | solution.py:17
  524.9 7.9 %copy-start.3 = (bf16[8,256,512]{2,1,0:T(8,128)(2,1)S(1)}, bf16[8,256,512]{2,1,0:T(8,128)(2,1)}, u32[]{:S(2)}) copy-start(bf16[8,256,512]{2,1,0:T(8,128)(2,1)} %copy-done.2) | copy-start | bytes 6291460
Sparse Core Ops, SparseCore 0:
  312.9 52.6 all-gather.2
